TPU v7x, 32 devices: a whole 2x2x4 slice. The times are simulated.
32 devices in a mesh: fs: 16 (over z, y, x), tp: 2 (over core).
Axes of the slice: x: 2, y: 2, z: 4, core: 2. Of those that a mesh axis runs over, the one named last changes fastest.
Arguments:
- saved_inputs: bfloat16 [2048, 4096], P('fs', 'tp'), may hold values from -6 to 6
- value_cotangent: bfloat16 [2048, 2048], P('fs'), may hold values from -0.1875 to 0.1875
- glu_output: bfloat16 [2048, 2048], P('fs', 'tp'), may hold values from -6 to 6
- conv_cotangent: bfloat16 [2048, 2048], P('fs', 'tp'), may hold values from -0.125 to 0.125
- factor: bfloat16 [4096, 256], P('tp'), may hold values from -0.09375 to 0.09375
- value_weight: float32 [2048, 4096], P('fs', 'tp'), may hold values from -3 to 3
- first_moment: float32 [2048, 256], P('fs', 'tp'), may hold values from -6 to 6
- second_moment: float32 [2048, 256], P('fs', 'tp'), may hold values from 0.25 to 4
- kernel: float32 [31, 2048], P(None, 'tp'), may hold values from -1 to 1
- kernel_first: float32 [31, 2048], P(None, 'tp'), may hold values from -6 to 6
- kernel_second: float32 [31, 2048], P(None, 'tp'), may hold values from 0.25 to 4
Outputs:
- new_value: float32 [2048, 4096], P('fs', 'tp')
- value_copy: bfloat16 [2048, 4096], P('fs', 'tp')
- value_step: float32 [2048, 4096], P('fs', 'tp')
- new_first: float32 [2048, 256], P('fs', 'tp')
- new_second: float32 [2048, 256], P('fs', 'tp')
- new_kernel: float32 [31, 2048], P(None, 'tp')
- new_kernel_first: float32 [31, 2048], P(None, 'tp')
- new_kernel_second: float32 [31, 2048], P(None, 'tp')
All inputs are finite; a program needn't handle non-finite values.
Results may differ from a plain program's by a relative error of at most 0.0055.
Values may be sent and summed in bfloat16 or wider, within the bound.
A program may use at most 64 MiB of HBM per device.

v0:
```python
import jax
import jax.numpy as jnp
from jax import lax
from jax.sharding import PartitionSpec as P

WIDTH = 4096


def from_behind(x, axis, by):
    peers = lax.axis_size(axis)
    pairs = [(i, i + by) for i in range(peers) if 0 <= i + by < peers]
    return lax.ppermute(x, axis, pairs)


def body(
    saved_inputs,
    value_cotangent,
    glu_output,
    conv_cotangent,
    factor,
    value_weight,
    first_moment,
    second_moment,
    kernel,
    kernel_first,
    kernel_second,
):
    highest = lax.Precision.HIGHEST
    factor_f = factor.astype(jnp.float32)
    partial_reduced = jnp.dot(saved_inputs, factor, preferred_element_type=jnp.float32)
    reduced = lax.psum_scatter(
        partial_reduced.astype(jnp.bfloat16), "tp", scatter_dimension=1, tiled=True
    ).astype(jnp.float32)
    upper_part = reduced.astype(jnp.bfloat16)
    lower_part = (reduced - upper_part.astype(jnp.float32)).astype(jnp.bfloat16)
    dims = (((0,), (0,)), ((), ()))
    upper_term = lax.dot_general(
        value_cotangent, upper_part, dims, preferred_element_type=jnp.float32
    )
    lower_term = lax.dot_general(
        value_cotangent, lower_part, dims, preferred_element_type=jnp.float32
    )
    projected = lax.psum_scatter(upper_term + lower_term, "fs", scatter_dimension=0, tiled=True)
    new_first = 0.8 * first_moment + 0.2 * projected
    new_second = 0.9 * second_moment + 0.1 * projected * projected
    direction = new_first / jnp.sqrt(new_second)
    full_direction = lax.all_gather(direction, "tp", axis=1, tiled=True)
    back_proj = jnp.dot(full_direction, factor_f.T, precision=highest)
    row_squares = lax.psum(jnp.sum(back_proj * back_proj, axis=1), "tp")
    value_step = back_proj / jnp.sqrt(row_squares / WIDTH + 0.01)[:, None]
    new_value = value_weight - 0.05 * value_step
    value_copy = new_value.astype(jnp.bfloat16)
    token_count = glu_output.shape[0]
    reach = kernel.shape[0] - 1
    halo_rows = from_behind(glu_output[token_count - reach :], "fs", 1)
    extended = jnp.concatenate([halo_rows, glu_output], axis=0).astype(jnp.float32)
    cotangent_f = conv_cotangent.astype(jnp.float32)
    pieces = []
    for offset in range(kernel.shape[0]):
        begin = reach - offset
        pieces.append(jnp.sum(extended[begin : begin + token_count] * cotangent_f, axis=0))
    local_grad = jnp.stack(pieces, axis=0)
    kernel_grad = lax.psum(local_grad, "fs")
    new_kernel_first = 0.8 * kernel_first + 0.2 * kernel_grad
    new_kernel_second = 0.9 * kernel_second + 0.1 * kernel_grad * kernel_grad
    new_kernel = kernel - 0.05 * new_kernel_first / jnp.sqrt(new_kernel_second)
    return (
        new_value,
        value_copy,
        value_step,
        new_first,
        new_second,
        new_kernel,
        new_kernel_first,
        new_kernel_second,
    )


def solution(mesh):
    placed = (
        P("fs", "tp"),
        P("fs", None),
        P("fs", "tp"),
        P("fs", "tp"),
        P("tp", None),
        P("fs", "tp"),
        P("fs", "tp"),
        P("fs", "tp"),
        P(None, "tp"),
        P(None, "tp"),
        P(None, "tp"),
    )
    return jax.shard_map(
        body,
        mesh=mesh,
        in_specs=placed,
        out_specs=(
            P("fs", "tp"),
            P("fs", "tp"),
            P("fs", "tp"),
            P("fs", "tp"),
            P("fs", "tp"),
            P(None, "tp"),
            P(None, "tp"),
            P(None, "tp"),
        ),
        check_vma=False,
    )
```

profile of v0, /device:TPU:0, one launch (start us, length us, event | category | flops | bytes accessed | tf_op | source)
XLA Modules:
  0.0 225.3 jit_solution(7543839092658024599)
XLA Ops:
  8.1 0.9 slice.96
  9.0 4.9 %collective-permute-start = (bf16[30,1024]{1,0:T(8,128)(2,1)S(1)}, bf16[30,1024]{1,0:T(8,128)(2,1)S(1)}, u32[]{:S(2)}, u32[]{:S(2)}) collective-permute-start(bf16[30,1024]{1,0:T(8,128)(2,1)S(1)} %slice.96), channel_id=1, source_target_pairs={{0,2},{2,4},{4,6},{6,8},{8,10},{10,12},{12,14},{14,16},{16,18},{18... | collective-permute-start | bytes 184328 | tf_op jit(solution)/shard_map/ppermute | solution.py:12
  13.9 1.4 convolution_convert_fusion
  15.3 0.7 copy.27
  16.2 0.8 copy-done.3
  17.0 1.1 fusion.31
  18.1 0.8 fusion.30
  18.9 2.7 %stack.127 = f32[31,1024]{1,0:T(8,128)} concatenate(f32[1,1024]{1,0:T(1,128)S(1)} %bitcast.75, f32[1,1024]{1,0:T(1,128)S(1)} %bitcast.46, f32[1,1024]{1,0:T(1,128)S(1)} %bitcast.47, f32[1,1024]{1,0:T(1,128)S(1)} %bitcast.48, f32[1,1024]{1,0:T(1,128)S(1)} %bitcast.49, f32[1,1024]{1,0:T(1,128)S(1)} %bitcast.50, f32[1,1024]{1,0:T(1,128)S(1)} %bitcast.51, f32[1,1024]{1,0:T(1,128)S(1)} %bitcast.52, ...), dimensions={0} | concatenate | bytes 253952 | tf_op jit(solution)/shard_map/stack | solution.py:62
  21.7 2.4 %reduce-scatter.7.cloned.1.call-done = bf16[128,128]{1,0:T(8,128)(2,1)} async-done(((bf16[256,128]{1,0:T(8,128)(2,1)}), bf16[128,128]{1,0:T(8,128)(2,1)}) %reduce-scatter.7.cloned.1.call-update) | async-done | bytes 32784
  24.1 0.9 copy.28
  25.0 0.3 fusion.34
  25.3 1.3 fusion
  26.6 0.8 copy-done.9
  27.6 0.1 copy.23
  27.7 100.1 %all-reduce.2.cloned.1.call-done = f32[31,1024]{1,0:T(8,128)} async-done(((f32[31,1024]{1,0:T(8,128)}), f32[31,1024]{1,0:T(8,128)}) %all-reduce.2.cloned.1.call-update) | async-done | bytes 126992 | tf_op jit(solution)/shard_map/psum | solution.py:63
  127.7 1.7 multiply_subtract_fusion.1
  129.4 78.8 %reduce-scatter.5.cloned.1.call-done = f32[128,128]{0,1:T(8,128)} async-done(((f32[2048,128]{0,1:T(8,128)}), f32[128,128]{0,1:T(8,128)}) %reduce-scatter.5.cloned.1.call-update) | async-done | bytes 65552 | tf_op jit(solution)/shard_map/reduce_scatter | solution.py:43
  208.2 0.9 rsqrt_multiply_fusion
  209.1 1.9 all_gather.3
  211.0 1.1 multiply_reduce_fusion
  212.1 2.5 %psum.14 = f32[128]{0:T(128)S(1)} all-reduce(f32[128]{0:T(128)S(1)} %get-tuple-element.64), channel_id=1, replica_groups=mesh['fs'=16,'tp'=2] {'tp'}, use_global_device_ids=true, to_apply=%region_3.0 | all-reduce | flops 128 | bytes 1024 | tf_op jit(solution)/shard_map/psum | solution.py:49
  214.5 0.7 copy.25
  215.3 0.7 copy.26
  216.0 1.8 fusion.37
  (30 shorter events, 0.4 us)
Async XLA Ops:
  8.0 5.9 %copy-start = (bf16[2048,256]{1,0:T(8,128)(2,1)S(1)}, bf16[2048,256]{1,0:T(8,128)(2,1)}, u32[]{:S(2)}) copy-start(bf16[2048,256]{1,0:T(8,128)(2,1)} %param.15) | copy-start | bytes 3145732
  8.0 16.1 %reduce-scatter.7.cloned.1.call-start = ((), (), s32[]{:S(2)}) async-start(), calls=%async_computation.4 | async-start | bytes 98304
  9.0 7.1 %collective-permute-start = (bf16[30,1024]{1,0:T(8,128)(2,1)S(1)}, bf16[30,1024]{1,0:T(8,128)(2,1)S(1)}, u32[]{:S(2)}, u32[]{:S(2)}) collective-permute-start(bf16[30,1024]{1,0:T(8,128)(2,1)S(1)} %slice.96), channel_id=1, source_target_pairs={{0,2},{2,4},{4,6},{6,8},{8,10},{10,12},{12,14},{14,16},{16,18},{18... | collective-permute-start | bytes 184328 | tf_op jit(solution)/shard_map/ppermute | solution.py:12
  13.9 2.2 copy-start.4
  16.1 1.0 copy-start.3
  16.1 111.7 %all-reduce.2.cloned.1.call-start = ((), (), s32[]{:S(2)}) async-start(), calls=%async_computation.3 | async-start | bytes 262144 | tf_op jit(solution)/shard_map/psum | solution.py:63
  18.9 6.1 %copy-start.1 = (bf16[128,2048]{1,0:T(8,128)(2,1)S(1)}, bf16[128,2048]{1,0:T(8,128)(2,1)}, u32[]{:S(2)}) copy-start(bf16[128,2048]{1,0:T(8,128)(2,1)} %param.12) | copy-start | bytes 1572868
  21.6 186.6 %reduce-scatter.5.cloned.1.call-start = ((), (), s32[]{:S(2)}) async-start(), calls=%async_computation.2 | async-start | bytes 1114112 | tf_op jit(solution)/shard_map/reduce_scatter | solution.py:43
  24.1 1.0 copy-start.8
  26.6 0.8 copy-start.9
  26.6 0.9 copy-start.10
  26.6 101.1 %copy-start.7 = (f32[31,1024]{1,0:T(8,128)S(1)}, f32[31,1024]{1,0:T(8,128)}, u32[]{:S(2)}) copy-start(f32[31,1024]{1,0:T(8,128)} %param.21) | copy-start | bytes 380932
  27.5 100.3 %copy-start.5 = (f32[31,1024]{1,0:T(8,128)S(1)}, f32[31,1024]{1,0:T(8,128)}, u32[]{:S(2)}) copy-start(f32[31,1024]{1,0:T(8,128)} %param.19) | copy-start | bytes 380932
  27.5 100.3 %copy-start.6 = (f32[31,1024]{1,0:T(8,128)S(1)}, f32[31,1024]{1,0:T(8,128)}, u32[]{:S(2)}) copy-start(f32[31,1024]{1,0:T(8,128)} %param.20) | copy-start | bytes 380932
  211.0 5.0 %copy-start.2 = (f32[128,2048]{1,0:T(8,128)S(1)}, f32[128,2048]{1,0:T(8,128)}, u32[]{:S(2)}) copy-start(f32[128,2048]{1,0:T(8,128)} %param.16) | copy-start | bytes 3145732
Sparse Core Ops, SparseCore 0:
  16.2 7.8 reduce-scatter.6
Sparse Core Ops, SparseCore 1:
  22.6 105.1 all-reduce.1
  130.4 77.7 reduce-scatter.4
where the time goes:
time: 226 us; the launch traced here: 225 us
  waiting for transfers between devices  181 us (80%)
  between operations  15.6 us (7%)
  local copies, waits for them, and re-layouts  8.54 us (4%)
  other arithmetic  6.33 us (3%)
  starting transfers between devices  5 us (2%)
  blocking collectives  4.37 us (2%)
  matrix products  4.05 us (2%)
    psum x1, waiting for transfers between devices, body(): kernel_grad = lax.psum(local_grad, 'fs')  100 us
    reduce_scatter x1, waiting for transfers between devices, body(): lax.psum_scatter(upper_term + lower_term, 'fs', scatter_dimension=0, tile...  78.8 us
    unnamed x28, local copies, waits for them, and re-layouts  4.95 us
    ppermute x1, starting transfers between devices, from_behind(): return lax.ppermute(x, axis, pairs)  4.87 us
  transfers between devices with their start and end apart: 4, of which 3 were waited for; matrix products, arithmetic and copies ran while one was open for 5% of the time, Pallas kernels for 0%

commit v1 on v0

--- a/solution.py
+++ b/solution.py
@@ -2,6 +2,7 @@
 import jax.numpy as jnp
 from jax import lax
 from jax.sharding import PartitionSpec as P
+from jax.lax import all_gather
 
 WIDTH = 4096
 
@@ -60,7 +61,7 @@
         begin = reach - offset
         pieces.append(jnp.sum(extended[begin : begin + token_count] * cotangent_f, axis=0))
     local_grad = jnp.stack(pieces, axis=0)
-    kernel_grad = lax.psum(local_grad, "fs")
+    kernel_grad = all_gather(local_grad, "fs").sum(axis=0)
     new_kernel_first = 0.8 * kernel_first + 0.2 * kernel_grad
     new_kernel_second = 0.9 * kernel_second + 0.1 * kernel_grad * kernel_grad
     new_kernel = kernel - 0.05 * new_kernel_first / jnp.sqrt(new_kernel_second)

time: 226 us -> 174 us (0.77)
  waiting for transfers between devices: 181 us -> 132 us
    psum x1 -> x0, waiting for transfers between devices: 100 us -> none  [body(): kernel_grad = lax.psum(local_grad, 'fs')]
    all_gather x0 -> x1, waiting for transfers between devices: none -> 50.5 us  [body(): kernel_grad = all_gather(local_grad, 'fs').sum(axis=0)]
    reduce_scatter x1, waiting for transfers between devices: 78.8 us -> 69.5 us  [body(): lax.psum_scatter(upper_term + lower_term, 'fs', scatter_dimension=0, tile...]
    unnamed x4, waiting for transfers between devices: 2.46 us -> 10.5 us
    unnamed x28 -> x26, local copies, waits for them, and re-layouts: 4.95 us -> 4.44 us
  transfers between devices with their start and end apart: 4 -> 4, of which waited for: 3 -> 4; matrix products, arithmetic and copies ran while one was open for 5% -> 6% of each run, Pallas kernels for 0% -> 0%
where the time goes in v1:
time: 174 us; the launch traced here: 173 us
  waiting for transfers between devices  132 us (76%)
  between operations  13.9 us (8%)
  other arithmetic  7.16 us (4%)
  local copies, waits for them, and re-layouts  7.12 us (4%)
  matrix products  4.77 us (3%)
  blocking collectives  4.35 us (2%)
  starting transfers between devices  3.71 us (2%)
    reduce_scatter x1, waiting for transfers between devices, body(): lax.psum_scatter(upper_term + lower_term, 'fs', scatter_dimension=0, tile...  69.5 us
    all_gather x1, waiting for transfers between devices, body(): kernel_grad = all_gather(local_grad, 'fs').sum(axis=0)  50.5 us
    unnamed x4, waiting for transfers between devices  10.5 us
    unnamed x26, local copies, waits for them, and re-layouts  4.44 us
    ppermute x1, starting transfers between devices, from_behind(): return lax.ppermute(x, axis, pairs)  3.58 us
  transfers between devices with their start and end apart: 4, of which 4 were waited for; matrix products, arithmetic and copies ran while one was open for 6% of the time, Pallas kernels for 0%

profile of v1, /device:TPU:0, one launch (start us, length us, event | category | flops | bytes accessed | tf_op | source)
XLA Modules:
  0.0 173.5 jit_solution(16806347754292297058)
XLA Ops:
  7.2 1.2 copy-done
  8.4 1.3 convolution_convert_fusion
  9.8 0.7 copy.27
  10.6 10.5 %reduce-scatter.7.cloned.1.call-done = bf16[128,128]{1,0:T(8,128)(2,1)} async-done(((bf16[256,128]{1,0:T(8,128)(2,1)}), bf16[128,128]{1,0:T(8,128)(2,1)}) %reduce-scatter.7.cloned.1.call-update) | async-done | bytes 32784
  21.1 0.9 copy.28
  21.9 1.0 fusion.34
  23.0 1.3 fusion
  24.4 3.6 %collective-permute-start = (bf16[30,1024]{1,0:T(8,128)(2,1)S(1)}, bf16[30,1024]{1,0:T(8,128)(2,1)S(1)}, u32[]{:S(2)}, u32[]{:S(2)}) collective-permute-start(bf16[30,1024]{1,0:T(8,128)(2,1)S(1)} %slice.96), channel_id=1, source_target_pairs={{0,2},{2,4},{4,6},{6,8},{8,10},{10,12},{12,14},{14,16},{16,18},{18... | collective-permute-start | bytes 184328 | tf_op jit(solution)/shard_map/ppermute | solution.py:13
  28.0 1.9 %collective-permute-done = bf16[30,1024]{1,0:T(8,128)(2,1)S(1)} collective-permute-done((bf16[30,1024]{1,0:T(8,128)(2,1)S(1)}, bf16[30,1024]{1,0:T(8,128)(2,1)S(1)}, u32[]{:S(2)}, u32[]{:S(2)}) %collective-permute-start) | collective-permute-done | bytes 61472 | tf_op jit(solution)/shard_map/ppermute | solution.py:13
  30.0 0.8 fusion.30
  30.8 1.1 fusion.31
  31.9 2.7 %stack.127 = f32[31,1024]{1,0:T(8,128)} concatenate(f32[1,1024]{1,0:T(1,128)S(1)} %bitcast.59, f32[1,1024]{1,0:T(1,128)S(1)} %bitcast.61, f32[1,1024]{1,0:T(1,128)S(1)} %bitcast.62, f32[1,1024]{1,0:T(1,128)S(1)} %bitcast.63, f32[1,1024]{1,0:T(1,128)S(1)} %bitcast.64, f32[1,1024]{1,0:T(1,128)S(1)} %bitcast.65, f32[1,1024]{1,0:T(1,128)S(1)} %bitcast.66, f32[1,1024]{1,0:T(1,128)S(1)} %bitcast.67, ...), dimensions={0} | concatenate | bytes 253952 | tf_op jit(solution)/shard_map/stack | solution.py:63
  34.6 0.1 copy.23
  34.8 69.5 %reduce-scatter.5.cloned.1.call-done = f32[128,128]{0,1:T(8,128)} async-done(((f32[2048,128]{0,1:T(8,128)}), f32[128,128]{0,1:T(8,128)}) %reduce-scatter.5.cloned.1.call-update) | async-done | bytes 65552 | tf_op jit(solution)/shard_map/reduce_scatter | solution.py:44
  104.3 0.9 rsqrt_multiply_fusion
  105.2 0.7 copy.26
  105.9 0.7 copy.25
  106.7 1.9 %all_gather.9 = f32[128,256]{0,1:T(8,128)S(1)} all-gather(f32[128,128]{0,1:T(8,128)S(1)} %get-tuple-element.61), channel_id=1, replica_groups=mesh['fs'=16,'tp'=2] {'tp'}, dimensions={1}, use_global_device_ids=true | all-gather | bytes 196608 | tf_op jit(solution)/shard_map/all_gather | solution.py:48
  108.6 1.1 multiply_reduce_fusion
  109.6 2.5 %psum.7 = f32[128]{0:T(128)S(1)} all-reduce(f32[128]{0:T(128)S(1)} %get-tuple-element.64), channel_id=1, replica_groups=mesh['fs'=16,'tp'=2] {'tp'}, use_global_device_ids=true, to_apply=%region_3.0 | all-reduce | flops 128 | bytes 1024 | tf_op jit(solution)/shard_map/psum | solution.py:50
  112.1 1.8 %fusion.37 = (bf16[128,2048]{1,0:T(8,128)(2,1)}, f32[128,2048]{1,0:T(8,128)}, f32[128,2048]{1,0:T(8,128)}) fusion(f32[128,2048]{1,0:T(8,128)S(1)} %copy-done.2, f32[128,2048]{1,0:T(8,128)S(1)} %get-tuple-element.65, f32[128]{0:T(128)S(1)} %add_sqrt_fusion), kind=kLoop, calls=%fused_computation.81 | loop fusion | flops 1048576 | bytes 4719104 | tf_op jit(solution)/shard_map/convert_element_type | solution.py:53
  114.0 50.5 %all-gather.4.cloned.1.call-done = f32[16,31,1024]{2,1,0:T(8,128)} async-done(((f32[1,31,1024]{2,1,0:T(8,128)}), f32[16,31,1024]{2,1,0:T(8,128)}) %all-gather.4.cloned.1.call-update) | async-done | bytes 2031632 | tf_op jit(solution)/shard_map/all_gather | solution.py:64
  164.4 1.7 reduce_sum.329
  166.2 0.8 multiply_subtract_fusion.1
  (29 shorter events, 0.4 us)
Async XLA Ops:
  7.2 1.2 copy-start
  7.2 14.7 %copy-start.1 = (bf16[128,2048]{1,0:T(8,128)(2,1)S(1)}, bf16[128,2048]{1,0:T(8,128)(2,1)}, u32[]{:S(2)}) copy-start(bf16[128,2048]{1,0:T(8,128)(2,1)} %param.12) | copy-start | bytes 1572868
  7.2 13.9 %reduce-scatter.7.cloned.1.call-start = ((), (), s32[]{:S(2)}) async-start(), calls=%async_computation.4 | async-start | bytes 98304
  10.5 93.8 %reduce-scatter.5.cloned.1.call-start = ((), (), s32[]{:S(2)}) async-start(), calls=%async_computation.2 | async-start | bytes 1114112 | tf_op jit(solution)/shard_map/reduce_scatter | solution.py:44
  23.0 1.4 copy-start.4
  23.0 7.0 %copy-start.3 = (bf16[128,1024]{1,0:T(8,128)(2,1)S(1)}, bf16[128,1024]{1,0:T(8,128)(2,1)}, u32[]{:S(2)}) copy-start(bf16[128,1024]{1,0:T(8,128)(2,1)} %param.14) | copy-start | bytes 786436
  24.3 140.1 %all-gather.4.cloned.1.call-start = ((), (), s32[]{:S(2)}) async-start(), calls=%async_computation.3 | async-start | bytes 2228224 | tf_op jit(solution)/shard_map/all_gather | solution.py:64
  24.4 5.5 %collective-permute-start = (bf16[30,1024]{1,0:T(8,128)(2,1)S(1)}, bf16[30,1024]{1,0:T(8,128)(2,1)S(1)}, u32[]{:S(2)}, u32[]{:S(2)}) collective-permute-start(bf16[30,1024]{1,0:T(8,128)(2,1)S(1)} %slice.96), channel_id=1, source_target_pairs={{0,2},{2,4},{4,6},{6,8},{8,10},{10,12},{12,14},{14,16},{16,18},{18... | collective-permute-start | bytes 184328 | tf_op jit(solution)/shard_map/ppermute | solution.py:13
  30.8 3.8 %copy-start.8 = (f32[128,128]{1,0:T(8,128)S(1)}, f32[128,128]{1,0:T(8,128)}, u32[]{:S(2)}) copy-start(f32[128,128]{1,0:T(8,128)} %param.17) | copy-start | bytes 196612
  30.8 3.9 %copy-start.9 = (f32[128,128]{1,0:T(8,128)S(1)}, f32[128,128]{1,0:T(8,128)}, u32[]{:S(2)}) copy-start(f32[128,128]{1,0:T(8,128)} %param.18) | copy-start | bytes 196612
  31.9 80.2 %copy-start.2 = (f32[128,2048]{1,0:T(8,128)S(1)}, f32[128,2048]{1,0:T(8,128)}, u32[]{:S(2)}) copy-start(f32[128,2048]{1,0:T(8,128)} %param.16) | copy-start | bytes 3145732
  114.0 52.2 %copy-start.5 = (f32[31,1024]{1,0:T(8,128)S(1)}, f32[31,1024]{1,0:T(8,128)}, u32[]{:S(2)}) copy-start(f32[31,1024]{1,0:T(8,128)} %param.19) | copy-start | bytes 380932
  114.0 52.2 %copy-start.6 = (f32[31,1024]{1,0:T(8,128)S(1)}, f32[31,1024]{1,0:T(8,128)}, u32[]{:S(2)}) copy-start(f32[31,1024]{1,0:T(8,128)} %param.20) | copy-start | bytes 380932
  114.0 52.2 %copy-start.7 = (f32[31,1024]{1,0:T(8,128)S(1)}, f32[31,1024]{1,0:T(8,128)}, u32[]{:S(2)}) copy-start(f32[31,1024]{1,0:T(8,128)} %param.21) | copy-start | bytes 380932
Sparse Core Ops, SparseCore 0:
  10.8 10.2 reduce-scatter.6
  24.4 79.8 reduce-scatter.4
  107.7 56.6 all-gather.3
